TPU v7x, 32 devices: a whole 2x2x4 slice. The times are simulated.
32 devices in a mesh: sp: 4 (over z), fs: 4 (over y, x), tp: 2 (over core).
Axes of the slice: x: 2, y: 2, z: 4, core: 2. Of those that a mesh axis runs over, the one named last changes fastest.
Arguments:
- tokens: bfloat16 [2048, 2048], P('sp', ('fs', 'tp')), may hold values from -6 to 6
- in_gain: float32 [2048], replicated, may hold values from 0.1 to 1.9
- conv_a_weight: bfloat16 [2048, 1024], P(None, ('fs', 'tp')), may hold values from -0.125 to 0.125
- conv_gate_weight: bfloat16 [2048, 1024], P(None, ('fs', 'tp')), may hold values from -0.125 to 0.125
- query_weight: bfloat16 [2048, 1024], P(None, ('fs', 'tp')), may hold values from -0.125 to 0.125
- key_weight: bfloat16 [2048, 1024], P(None, ('fs', 'tp')), may hold values from -0.125 to 0.125
- value_weight: bfloat16 [2048, 1024], P(None, ('fs', 'tp')), may hold values from -0.125 to 0.125
- conv_taps: bfloat16 [31, 1024], replicated, may hold values from -3 to 3
- conv_norm_gain: float32 [1024], replicated, may hold values from 0.1 to 1.9
- break_shift: bfloat16 [16, 2048], P(('fs', 'tp'), 'sp'), may hold values from -20 to 1
- conv_out_gain: float32 [1024], replicated, may hold values from 0.1 to 1.9
- attn_out_gain: float32 [1024], replicated, may hold values from 0.1 to 1.9
- out_weight: bfloat16 [2048, 2048], P(None, ('fs', 'tp')), may hold values from -0.125 to 0.125
Outputs:
- mixed: bfloat16 [2048, 2048], P('sp', ('fs', 'tp'))
All inputs are finite; a program needn't handle non-finite values.
Results may differ from a plain program's by a relative error of at most 0.0078.
Values may be sent and summed in bfloat16 or wider, within the bound.
A program may use at most 128 MiB of HBM per device.

v0:
```python
import jax
import jax.numpy as jnp
from jax import lax
from jax.sharding import PartitionSpec as P

HEAD_DIM = 64
epsilon = 1e-06


def passed_along(shard, axis, by):
    count = lax.axis_size(axis)
    pairs = [(i, i + by) for i in range(count) if 0 <= i + by < count]
    return lax.ppermute(shard, axis, pairs)


def per_device(
    tokens,
    in_gain,
    conv_a_weight,
    conv_gate_weight,
    query_weight,
    key_weight,
    value_weight,
    conv_taps,
    conv_norm_gain,
    break_shift,
    conv_out_gain,
    attn_out_gain,
    out_weight,
):
    rows_here = tokens.shape[0]
    model_width = in_gain.shape[0]
    channels = model_width // 2
    local_width = conv_a_weight.shape[1]
    heads_here = break_shift.shape[0]
    group_index = lax.axis_index(("fs", "tp"))
    shard_index = lax.axis_index("sp")
    stacked = jnp.concatenate(
        (conv_a_weight, conv_gate_weight, query_weight, key_weight, value_weight), axis=1
    )
    segment = lax.all_gather(tokens, ("fs", "tp"), axis=1, tiled=True)
    segment_wide = segment.astype(jnp.float32)
    scaled = (segment_wide * in_gain[None, :]).astype(jnp.bfloat16)
    totals = jnp.dot(scaled, stacked, preferred_element_type=jnp.float32)
    totals, squares = (totals, jnp.sum(segment_wide * segment_wide, axis=1))
    input_scale = lax.rsqrt(squares / model_width + epsilon)
    projected = (totals * input_scale[:, None]).astype(jnp.bfloat16)
    conv_a = projected[:, :local_width]
    conv_gate = projected[:, local_width : 2 * local_width]
    query = projected[:, 2 * local_width : 3 * local_width]
    key = projected[:, 3 * local_width : 4 * local_width]
    value = projected[:, 4 * local_width :]
    gated_input = conv_a.astype(jnp.float32) * jax.nn.sigmoid(conv_gate.astype(jnp.float32))
    reach_rows = conv_taps.shape[0] - 1
    earlier = passed_along(gated_input[rows_here - reach_rows :], "sp", 1)
    padded = jnp.concatenate((earlier, gated_input), axis=0)
    tap_values = lax.dynamic_slice_in_dim(
        conv_taps, group_index * local_width, local_width, 1
    ).astype(jnp.float32)
    conv_out = jnp.zeros((rows_here, local_width), jnp.float32)
    for offset in range(reach_rows + 1):
        conv_out = conv_out + tap_values[offset][None, :] * padded[offset : offset + rows_here]
    first_sum, second_sum = lax.psum(
        (jnp.sum(conv_out, axis=1), jnp.sum(conv_out * conv_out, axis=1)), ("fs", "tp")
    )
    row_mean = first_sum / channels
    row_spread = second_sum / channels - row_mean * row_mean
    centered = conv_out - row_mean[:, None]
    norm_gain = lax.dynamic_slice_in_dim(conv_norm_gain, group_index * local_width, local_width, 0)
    normed = centered * lax.rsqrt(row_spread + epsilon)[:, None] * norm_gain[None, :]
    conv_mixed = jax.nn.silu(normed).astype(jnp.bfloat16)
    queries = query.reshape(rows_here, heads_here, HEAD_DIM)
    query_pos = shard_index * rows_here + jnp.arange(rows_here, dtype=jnp.int32)
    score_scale = HEAD_DIM ** (-0.5)

    def attend(running, key_rows, value_rows, shift_rows, start_pos):
        outputs, behind = running
        piece_rows = key_rows.shape[0]
        key_heads = key_rows.reshape(piece_rows, heads_here, HEAD_DIM)
        value_heads = value_rows.reshape(piece_rows, heads_here, HEAD_DIM)
        scores = (
            jnp.einsum("qhd,khd->hqk", queries, key_heads, preferred_element_type=jnp.float32)
            * score_scale
        )
        scores = scores + shift_rows.astype(jnp.float32)[:, None, :]
        key_pos = start_pos + jnp.arange(piece_rows, dtype=jnp.int32)
        allowed = ((key_pos[None, :] < query_pos[:, None]) & (key_pos[None, :] >= 0))[None]
        log_fail = jnp.where(allowed, jax.nn.log_sigmoid(-scores), 0.0)
        later_sum = lax.cumsum(log_fail, axis=2, reverse=True) - log_fail + behind[:, :, None]
        weights = jnp.where(allowed, jnp.exp(jax.nn.log_sigmoid(scores) + later_sum), 0.0).astype(
            jnp.bfloat16
        )
        outputs = outputs + jnp.einsum(
            "hqk,khd->qhd", weights, value_heads, preferred_element_type=jnp.float32
        )
        return (outputs, behind + jnp.sum(log_fail, axis=2))

    start_state = (
        jnp.zeros((rows_here, heads_here, HEAD_DIM), jnp.float32),
        jnp.zeros((heads_here, rows_here), jnp.float32),
    )
    all_keys, all_values, all_shifts = (
        lax.all_gather(key, "sp", axis=0, tiled=True),
        lax.all_gather(value, "sp", axis=0, tiled=True),
        lax.all_gather(break_shift, "sp", axis=1, tiled=True),
    )
    sp_count = lax.axis_size("sp")
    grouped = 1
    while grouped * 2 * rows_here <= 1024 and sp_count % (grouped * 2) == 0:
        grouped = grouped * 2
    block_rows = grouped * rows_here
    last_block = (shard_index * rows_here + rows_here - 1) // block_rows

    def advance(counter, running):
        begin_row = (last_block - counter) * block_rows
        key_rows = lax.dynamic_slice_in_dim(all_keys, begin_row, block_rows, 0)
        value_rows = lax.dynamic_slice_in_dim(all_values, begin_row, block_rows, 0)
        shift_rows = lax.dynamic_slice_in_dim(all_shifts, begin_row, block_rows, 1)
        return attend(running, key_rows, value_rows, shift_rows, begin_row)

    outputs, behind = lax.fori_loop(0, last_block + 1, advance, start_state)
    attn_mixed = outputs.reshape(rows_here, heads_here * HEAD_DIM).astype(jnp.bfloat16)
    conv_piece = lax.all_gather(conv_mixed, ("fs", "tp"), axis=1, tiled=True)
    attn_piece = lax.all_gather(attn_mixed, ("fs", "tp"), axis=1, tiled=True)
    piece_width = conv_piece.shape[1]
    conv_wide = conv_piece.astype(jnp.float32)
    attn_wide = attn_piece.astype(jnp.float32)
    conv_scaled = (conv_wide * conv_out_gain[None, :]).astype(jnp.bfloat16)
    attn_scaled = (attn_wide * attn_out_gain[None, :]).astype(jnp.bfloat16)
    conv_rows = lax.slice_in_dim(out_weight, 0, piece_width, axis=0)
    attn_rows = lax.dynamic_slice_in_dim(out_weight, channels, piece_width, 0)
    conv_total = jnp.dot(conv_scaled, conv_rows, preferred_element_type=jnp.float32)
    attn_total = jnp.dot(attn_scaled, attn_rows, preferred_element_type=jnp.float32)
    conv_squares = jnp.sum(conv_wide * conv_wide, axis=1)
    attn_squares = jnp.sum(attn_wide * attn_wide, axis=1)
    conv_total, attn_total, conv_squares, attn_squares = (
        conv_total,
        attn_total,
        conv_squares,
        attn_squares,
    )
    conv_scale = lax.rsqrt(conv_squares / channels + epsilon)
    attn_scale = lax.rsqrt(attn_squares / channels + epsilon)
    mixed = conv_total * conv_scale[:, None] + attn_total * attn_scale[:, None]
    return mixed.astype(jnp.bfloat16)


def solution(mesh):
    return jax.shard_map(
        per_device,
        mesh=mesh,
        in_specs=(
            P("sp", ("fs", "tp")),
            P(),
            P(None, ("fs", "tp")),
            P(None, ("fs", "tp")),
            P(None, ("fs", "tp")),
            P(None, ("fs", "tp")),
            P(None, ("fs", "tp")),
            P(),
            P(),
            P(("fs", "tp"), "sp"),
            P(),
            P(),
            P(None, ("fs", "tp")),
        ),
        out_specs=P("sp", ("fs", "tp")),
        check_vma=False,
    )
```

profile of v0, /device:TPU:0, one launch (start us, length us, event | category | flops | bytes accessed | tf_op | source)
XLA Modules:
  0.0 200.8 jit_solution(11392080675907995282)
XLA Ops:
  6.5 0.7 all-gather.4.cloned.1.call-update
  7.3 13.8 %all_gather.22 = bf16[2,2048]{1,0:T(2,128)(2,1)S(1)} all-gather(bf16[2,512]{1,0:T(2,128)(2,1)} %param.24), channel_id=1, replica_groups=mesh['sp'=4,'fs'=4,'tp'=2] {'sp'}, dimensions={1}, use_global_device_ids=true | all-gather | bytes 10240 | tf_op jit(solution)/shard_map/all_gather | solution.py:105
  21.1 1.9 constant_dynamic-update-slice_fusion.4
  23.0 1.9 constant_dynamic-update-slice_fusion.3
  24.9 1.9 constant_dynamic-update-slice_fusion.2
  26.9 1.9 constant_dynamic-update-slice_fusion.1
  28.8 0.9 constant_dynamic-update-slice_fusion
  29.6 10.4 %all-gather.4.cloned.1.call-done = bf16[512,2048]{1,0:T(8,128)(2,1)} async-done(((bf16[512,256]{1,0:T(8,128)(2,1)}), bf16[512,2048]{1,0:T(8,128)(2,1)}) %all-gather.4.cloned.1.call-update) | async-done | bytes 2097168 | tf_op jit(solution)/shard_map/all_gather | solution.py:41
  40.1 2.1 %fusion.19 = f32[512]{0:T(512)S(1)} fusion(bf16[512,2048]{1,0:T(8,128)(2,1)} %all-gather.4.cloned.1.call-done), kind=kLoop, calls=%fused_computation.37 | loop fusion | flops 3145216 | bytes 2099200 | tf_op jit(solution)/shard_map/reduce_sum | solution.py:45
  42.2 4.2 %fusion.30 = bf16[512,640]{1,0:T(8,128)(2,1)S(1)} fusion(bf16[2048,640]{1,0:T(8,128)(2,1)} %constant_dynamic-update-slice_fusion, bf16[512,2048]{1,0:T(8,128)(2,1)} %all-gather.4.cloned.1.call-done, f32[2048]{0:T(1024)S(1)} %copy-done.4, f32[512]{0:T(512)S(1)} %add_rsqrt_fusion.3), kind=kOutput, calls=%fused_computation.78 | convolution fusion | flops 1345978368 | bytes 5384192 | tf_op jit(solution)/shard_map/dot_general | solution.py:44
  46.4 16.1 %all_gather.20 = bf16[2048,128]{1,0:T(8,128)(2,1)S(1)} all-gather(bf16[512,128]{1,0:T(8,128)(2,1)S(1)} %get-tuple-element.135), channel_id=1, replica_groups=mesh['sp'=4,'fs'=4,'tp'=2] {'sp'}, dimensions={0}, use_global_device_ids=true | all-gather | bytes 655360 | tf_op jit(solution)/shard_map/all_gather | solution.py:104
  62.5 16.0 %all_gather.21 = bf16[2048,128]{1,0:T(8,128)(2,1)S(1)} all-gather(bf16[512,128]{1,0:T(8,128)(2,1)S(1)} %get-tuple-element.134), channel_id=1, replica_groups=mesh['sp'=4,'fs'=4,'tp'=2] {'sp'}, dimensions={0}, use_global_device_ids=true | all-gather | bytes 655360 | tf_op jit(solution)/shard_map/all_gather | solution.py:103
  78.7 31.2 %while.13 = (s32[]{:T(128)}, f32[512,2,64]{0,2,1:T(8,128)S(1)}, f32[2,512]{1,0:T(2,128)S(1)}, s32[]{:T(128)}, s32[]{:T(128)}, /*index=5*/bf16[2048,128]{1,0:T(8,...) while((s32[]{:T(128)}, f32[512,2,64]{0,2,1:T(8,128)S(1)}, ...), condition=%wide.region_10.11_spmd.clone, body=%wide.region_6.10_spmd.clone.sunk | while | flops 439489024 | bytes 84838688 | solution.py:121
  79.2 0.8 compare_and_fusion.2
  80.2 5.1 %fusion.152 = (f32[2,512]{1,0:T(2,128)S(1)}, f32[2,512,1024]{1,2,0:T(8,128)S(1)}, f32[2,1024,512]{2,1,0:T(8,128)}) fusion(f32[2,1024]{1,0:T(2,128)S(1)} %dynamic-slice_convert_fusion.3, pred[512,1024]{0,1:T(8,128)(4,1)S(1)} %compare_and_fusion.2, bf16[1024,2,64]{0,2,1:T(8,128)(2,1)S(1)} %bitcast.133, bf16[512,2,64]{0,2,1:T(8,128)(2,1)S(1)} %get-tuple-element.278), kind=kOutput, calls=%fused_computation.33.clone.1 | convolution fusion | flops 145751040 | bytes 9318400 | tf_op jit(solution)/shard_map/while/body/qhd,khd->hqk/dot_general | solution.py:82
  85.2 10.1 %fusion.153 = f32[2,512,8,128]{1,2,3,0:T(8,128)S(1)} fusion(f32[2,512,8,128]{1,3,2,0:T(8,128)S(1)} %bitcast.131), kind=kOutput, calls=%fused_computation.19.clone.1 | output fusion | flops 133169152 | bytes 8388608 | tf_op jit(solution)/shard_map/reduce-window
  95.3 2.0 copy-done
  97.4 2.7 %broadcast_add_fusion.2 = f32[2,512,8,128]{1,2,3,0:T(8,128)S(1)} fusion(f32[2,512,8,128]{1,2,3,0:T(8,128)} %copy-done, f32[2,512,8]{1,2,0:T(8,128)S(1)} %slice.847), kind=kLoop, calls=%fused_computation.22.clone.1 | loop fusion | flops 1048576 | bytes 8421376 | tf_op jit(solution)/shard_map/reduce_window_sum | solution.py:89
  100.1 2.4 %copy.38 = f32[2,512,8,128]{1,3,2,0:T(8,128)S(1)} copy(f32[2,512,8,128]{1,2,3,0:T(8,128)S(1)} %broadcast_add_fusion.2) | data formatting | bytes 8388608 | tf_op jit(solution)/shard_map/reduce_window_sum | solution.py:89
  102.5 6.9 %fusion.154 = bf16[2,512,1024]{1,2,0:T(8,128)(2,1)S(1)} fusion(f32[2,512,8,128]{1,3,2,0:T(8,128)S(1)} %copy.38, f32[2,1024,512]{2,1,0:T(8,128)S(1)} %copy-done.1, f32[2,512]{1,0:T(2,128)S(1)} %get-tuple-element.258, f32[2,1024]{1,0:T(2,128)S(1)} %dynamic-slice_convert_fusion.3, pred[512,1024]{0,1:T(8,128)(4,1)S(1)} %compare_and_fusion.2), kind=kLoop, calls=%fused_computation.7.clone.1 | loop fusion | flops 24117248 | bytes 11022336 | tf_op jit(solution)/shard_map/while/body/convert_element_type | solution.py:90
  110.7 0.7 dynamic-slice_convert_fusion.1
  111.5 3.2 %collective-permute-start = (f32[30,128]{1,0:T(8,128)S(1)}, f32[30,128]{1,0:T(8,128)S(1)}, u32[]{:S(2)}, u32[]{:S(2)}) collective-permute-start(f32[30,128]{1,0:T(8,128)S(1)} %slice.285), channel_id=1, source_target_pairs={{0,8},{8,16},{16,24},{1,9},{9,17},{17,25},{2,10},{10,18},{18,26},{... | collective-permute-start | bytes 46088 | tf_op jit(solution)/shard_map/ppermute | solution.py:13
  114.7 0.8 dynamic_slice.19
  115.9 1.1 fusion.130
  117.0 11.8 %all-reduce = (f32[512]{0:T(512)S(1)}, f32[512]{0:T(512)S(1)}) all-reduce(f32[512]{0:T(512)S(1)} %get-tuple-element.104, f32[512]{0:T(512)S(1)} %get-tuple-element.103), channel_id=1, replica_groups=mesh['sp'=4,'fs'=4,'tp'=2] {'fs','tp'}, use_global_device_ids=true, to_apply=%region_4.0 | all-reduce | flops 1024 | bytes 8192 | tf_op jit(solution)/shard_map/psum | solution.py:63
  128.8 0.9 multiply_convert_fusion
  129.7 35.2 %all-gather.8.cloned.1.call-done = bf16[512,1024]{0,1:T(8,128)(2,1)} async-done(((bf16[512,128]{0,1:T(8,128)(2,1)}), bf16[512,1024]{0,1:T(8,128)(2,1)}) %all-gather.8.cloned.1.call-update) | async-done | bytes 1048592 | tf_op jit(solution)/shard_map/all_gather | solution.py:124
  164.9 1.5 fusion.23
  166.4 2.0 %convolution_multiply_fusion = f32[512,256]{1,0:T(8,128)S(1)} fusion(bf16[512,1024]{0,1:T(8,128)(2,1)} %all-gather.8.cloned.1.call-done, f32[1024]{0:T(1024)S(1)} %copy-done.5, bf16[2048,256]{1,0:T(8,128)(2,1)} %param.27, f32[512]{0:T(512)S(1)} %add_rsqrt_fusion), kind=kOutput, calls=%fused_computation.79 | convolution fusion | flops 270139392 | bytes 2103296 | tf_op jit(solution)/shard_map/dot_general | solution.py:133
  168.5 21.8 %all-gather.6.cloned.1.call-done = bf16[512,1024]{1,0:T(8,128)(2,1)} async-done(((bf16[512,128]{1,0:T(8,128)(2,1)}), bf16[512,1024]{1,0:T(8,128)(2,1)}) %all-gather.6.cloned.1.call-update) | async-done | bytes 1048592 | tf_op jit(solution)/shard_map/all_gather | solution.py:123
  190.3 1.5 fusion.21
  191.8 2.4 %fusion.34 = bf16[512,256]{1,0:T(8,128)(2,1)} fusion(f32[512,256]{1,0:T(8,128)S(1)} %convolution_multiply_fusion, bf16[512,1024]{1,0:T(8,128)(2,1)} %all-gather.6.cloned.1.call-done, f32[1024]{0:T(1024)S(1)} %copy-done.6, bf16[2048,256]{1,0:T(8,128)(2,1)S(1)} %copy-done.3, f32[512]{0:T(512)S(1)} %add_rsqrt_fusion.1), kind=kOutput, calls=%fused_computation.82 | convolution fusion | flops 270401536 | bytes 2365440 | tf_op jit(solution)/shard_map/dot_general | solution.py:132
  (44 shorter events, 2.5 us)
Async XLA Ops:
  6.5 22.2 %copy-start.2 = (bf16[2048,128]{1,0:T(8,128)(2,1)S(1)}, bf16[2048,128]{1,0:T(8,128)(2,1)}, u32[]{:S(2)}) copy-start(bf16[2048,128]{1,0:T(8,128)(2,1)} %param.21) | copy-start | bytes 1572868
  6.5 35.6 %copy-start.4 = (f32[2048]{0:T(1024)S(1)}, f32[2048]{0:T(1024)}, u32[]{:S(2)}) copy-start(f32[2048]{0:T(1024)} %param.16) | copy-start | bytes 24580
  6.5 33.5 %all-gather.4.cloned.1.call-start = ((), (), s32[]{:S(2)}) async-start(), calls=%async_computation | async-start | bytes 2359296 | tf_op jit(solution)/shard_map/all_gather | solution.py:41
  7.3 157.6 %all-gather.8.cloned.1.call-start = ((), (), s32[]{:S(2)}) async-start(), calls=%async_computation.2 | async-start | bytes 1179648 | tf_op jit(solution)/shard_map/all_gather | solution.py:124
  78.7 87.8 %copy-start.5 = (f32[1024]{0:T(1024)S(1)}, f32[1024]{0:T(1024)}, u32[]{:S(2)}) copy-start(f32[1024]{0:T(1024)} %param.26) | copy-start | bytes 12292
  95.3 2.0 copy-start
  100.1 2.4 %copy-start.1 = (f32[2,1024,512]{2,1,0:T(8,128)S(1)}, f32[2,1024,512]{2,1,0:T(8,128)}, u32[]{:S(2)}) copy-start(f32[2,1024,512]{2,1,0:T(8,128)} %get-tuple-element.239) | copy-start | bytes 12582916 | tf_op jit(solution)/shard_map/while
  109.9 81.9 %copy-start.3 = (bf16[2048,256]{1,0:T(8,128)(2,1)S(1)}, bf16[2048,256]{1,0:T(8,128)(2,1)}, u32[]{:S(2)}) copy-start(bf16[2048,256]{1,0:T(8,128)(2,1)} %param.27) | copy-start | bytes 3145732
  109.9 81.9 %copy-start.6 = (f32[1024]{0:T(1024)S(1)}, f32[1024]{0:T(1024)}, u32[]{:S(2)}) copy-start(f32[1024]{0:T(1024)} %param.25) | copy-start | bytes 12292
  110.6 79.7 %all-gather.6.cloned.1.call-start = ((), (), s32[]{:S(2)}) async-start(), calls=%async_computation.1 | async-start | bytes 1179648 | tf_op jit(solution)/shard_map/all_gather | solution.py:123
  111.5 4.4 %collective-permute-start = (f32[30,128]{1,0:T(8,128)S(1)}, f32[30,128]{1,0:T(8,128)S(1)}, u32[]{:S(2)}, u32[]{:S(2)}) collective-permute-start(f32[30,128]{1,0:T(8,128)S(1)} %slice.285), channel_id=1, source_target_pairs={{0,8},{8,16},{16,24},{1,9},{9,17},{17,25},{2,10},{10,18},{18,26},{... | collective-permute-start | bytes 46088 | tf_op jit(solution)/shard_map/ppermute | solution.py:13
Sparse Core Ops, SparseCore 0:
  9.2 30.8 all-gather.3
  110.7 54.1 all-gather.7
  166.8 23.4 all-gather.5
where the time goes:
time: 201 us
  waiting for transfers between devices  68.6 us (34%)
  blocking collectives  57.7 us (29%)
  other arithmetic  29.1 us (14%)
  local copies, waits for them, and re-layouts  14.3 us (7%)
  matrix products  14.1 us (7%)
  between operations  13.3 us (7%)
  starting transfers between devices  3.27 us (2%)
    all_gather x1, waiting for transfers between devices, per_device(): attn_piece = lax.all_gather(attn_mixed, ('fs', 'tp'), axis=1, tiled=True)  35.2 us
    all_gather x1, waiting for transfers between devices, per_device(): conv_piece = lax.all_gather(conv_mixed, ('fs', 'tp'), axis=1, tiled=True)  21.8 us
    all_gather x1, blocking collectives, per_device(): lax.all_gather(value, 'sp', axis=0, tiled=True)  16.1 us
    all_gather x1, blocking collectives, per_device(): lax.all_gather(key, 'sp', axis=0, tiled=True)  16 us
    all_gather x1, blocking collectives, per_device(): lax.all_gather(break_shift, 'sp', axis=1, tiled=True)  13.8 us
    psum x1, blocking collectives, per_device(): lax.psum((jnp.sum(conv_out, axis=1), jnp.sum(conv_out * conv_out, axis=1)...  11.8 us
    all_gather x1, waiting for transfers between devices, per_device(): segment = lax.all_gather(tokens, ('fs', 'tp'), axis=1, tiled=True)  10.4 us
    another operation x2, other arithmetic  10.1 us
  transfers between devices with their start and end apart: 4, of which 4 were waited for; matrix products, arithmetic and copies ran while one was open for 8% of the time, Pallas kernels for 0%

commit v1 on v0

--- a/solution.py
+++ b/solution.py
@@ -5,6 +5,11 @@
 
 HEAD_DIM = 64
 epsilon = 1e-06
+
+
+def gather_blocks(x, axis, along):
+    blocks = lax.all_gather(x, axis)
+    return jnp.concatenate(blocks, axis=along)
 
 
 def passed_along(shard, axis, by):
@@ -102,7 +107,7 @@
     all_keys, all_values, all_shifts = (
         lax.all_gather(key, "sp", axis=0, tiled=True),
         lax.all_gather(value, "sp", axis=0, tiled=True),
-        lax.all_gather(break_shift, "sp", axis=1, tiled=True),
+        gather_blocks(break_shift, "sp", 1),
     )
     sp_count = lax.axis_size("sp")
     grouped = 1

time: 201 us -> 201 us (level)
  no operation moved by 1% of the time
where the time goes in v1:
time: 201 us
  waiting for transfers between devices  68.6 us (34%)
  blocking collectives  57.7 us (29%)
  other arithmetic  29.1 us (14%)
  local copies, waits for them, and re-layouts  14.3 us (7%)
  matrix products  14.1 us (7%)
  between operations  13.3 us (7%)
  starting transfers between devices  3.27 us (2%)
    all_gather x1, waiting for transfers between devices, per_device(): attn_piece = lax.all_gather(attn_mixed, ('fs', 'tp'), axis=1, tiled=True)  35.2 us
    all_gather x1, waiting for transfers between devices, per_device(): conv_piece = lax.all_gather(conv_mixed, ('fs', 'tp'), axis=1, tiled=True)  21.8 us
    all_gather x1, blocking collectives, per_device(): lax.all_gather(value, 'sp', axis=0, tiled=True)  16.1 us
    all_gather x1, blocking collectives, per_device(): lax.all_gather(key, 'sp', axis=0, tiled=True)  16 us
    all_gather x1, blocking collectives, gather_blocks(): blocks = lax.all_gather(x, axis)  13.8 us
    psum x1, blocking collectives, per_device(): lax.psum((jnp.sum(conv_out, axis=1), jnp.sum(conv_out * conv_out, axis=1)...  11.8 us
    all_gather x1, waiting for transfers between devices, per_device(): segment = lax.all_gather(tokens, ('fs', 'tp'), axis=1, tiled=True)  10.4 us
    another operation x2, other arithmetic  10.1 us
  transfers between devices with their start and end apart: 4, of which 4 were waited for; matrix products, arithmetic and copies ran while one was open for 8% of the time, Pallas kernels for 0%

profile of v1, /device:TPU:0, one launch (start us, length us, event | category | flops | bytes accessed | tf_op | source)
XLA Modules:
  0.0 200.8 jit_solution(3201915320007578196)
XLA Ops:
  6.5 0.7 all-gather.6.cloned.1.call-update
  7.3 13.8 %all-gather.1 = bf16[4,2,512]{2,1,0:T(2,128)(2,1)S(1)} all-gather(bf16[1,2,512]{2,1,0:T(2,128)(2,1)} %bitcast.141), channel_id=2, replica_groups=mesh['sp'=4,'fs'=4,'tp'=2] {'sp'}, dimensions={0}, use_global_device_ids=true | all-gather | bytes 10240 | tf_op jit(solution)/shard_map/all_gather | solution.py:11
  21.1 1.9 constant_dynamic-update-slice_fusion.4
  23.0 1.9 constant_dynamic-update-slice_fusion.3
  24.9 1.9 constant_dynamic-update-slice_fusion.2
  26.9 1.9 constant_dynamic-update-slice_fusion.1
  28.8 0.9 constant_dynamic-update-slice_fusion
  29.6 10.4 %all-gather.6.cloned.1.call-done = bf16[512,2048]{1,0:T(8,128)(2,1)} async-done(((bf16[512,256]{1,0:T(8,128)(2,1)}), bf16[512,2048]{1,0:T(8,128)(2,1)}) %all-gather.6.cloned.1.call-update) | async-done | bytes 2097168 | tf_op jit(solution)/shard_map/all_gather | solution.py:46
  40.1 2.1 %fusion.19 = f32[512]{0:T(512)S(1)} fusion(bf16[512,2048]{1,0:T(8,128)(2,1)} %all-gather.6.cloned.1.call-done), kind=kLoop, calls=%fused_computation.37 | loop fusion | flops 3145216 | bytes 2099200 | tf_op jit(solution)/shard_map/reduce_sum | solution.py:50
  42.2 4.2 %fusion.30 = bf16[512,640]{1,0:T(8,128)(2,1)S(1)} fusion(bf16[2048,640]{1,0:T(8,128)(2,1)} %constant_dynamic-update-slice_fusion, bf16[512,2048]{1,0:T(8,128)(2,1)} %all-gather.6.cloned.1.call-done, f32[2048]{0:T(1024)S(1)} %copy-done.4, f32[512]{0:T(512)S(1)} %add_rsqrt_fusion.3), kind=kOutput, calls=%fused_computation.78 | convolution fusion | flops 1345978368 | bytes 5384192 | tf_op jit(solution)/shard_map/dot_general | solution.py:49
  46.4 16.1 %all_gather.23 = bf16[2048,128]{1,0:T(8,128)(2,1)S(1)} all-gather(bf16[512,128]{1,0:T(8,128)(2,1)S(1)} %get-tuple-element.145), channel_id=1, replica_groups=mesh['sp'=4,'fs'=4,'tp'=2] {'sp'}, dimensions={0}, use_global_device_ids=true | all-gather | bytes 655360 | tf_op jit(solution)/shard_map/all_gather | solution.py:109
  62.5 16.0 %all_gather.24 = bf16[2048,128]{1,0:T(8,128)(2,1)S(1)} all-gather(bf16[512,128]{1,0:T(8,128)(2,1)S(1)} %get-tuple-element.144), channel_id=1, replica_groups=mesh['sp'=4,'fs'=4,'tp'=2] {'sp'}, dimensions={0}, use_global_device_ids=true | all-gather | bytes 655360 | tf_op jit(solution)/shard_map/all_gather | solution.py:108
  78.7 31.2 %while.13 = (s32[]{:T(128)}, f32[512,2,64]{0,2,1:T(8,128)S(1)}, f32[2,512]{1,0:T(2,128)S(1)}, s32[]{:T(128)}, s32[]{:T(128)}, /*index=5*/bf16[2048,128]{1,0:T(8,...) while((s32[]{:T(128)}, f32[512,2,64]{0,2,1:T(8,128)S(1)}, ...), condition=%wide.region_10.11_spmd.clone, body=%wide.region_6.10_spmd.clone.sunk | while | flops 439489024 | bytes 84838688 | solution.py:126
  79.2 0.8 compare_and_fusion.2
  80.2 5.1 %fusion.152 = (f32[2,512]{1,0:T(2,128)S(1)}, f32[2,512,1024]{1,2,0:T(8,128)S(1)}, f32[2,1024,512]{2,1,0:T(8,128)}) fusion(f32[2,1024]{1,0:T(2,128)S(1)} %dynamic-slice_convert_fusion.3, pred[512,1024]{0,1:T(8,128)(4,1)S(1)} %compare_and_fusion.2, bf16[1024,2,64]{0,2,1:T(8,128)(2,1)S(1)} %bitcast.137, bf16[512,2,64]{0,2,1:T(8,128)(2,1)S(1)} %get-tuple-element.288), kind=kOutput, calls=%fused_computation.33.clone.1 | convolution fusion | flops 145751040 | bytes 9318400 | tf_op jit(solution)/shard_map/while/body/qhd,khd->hqk/dot_general | solution.py:87
  85.2 10.1 %fusion.153 = f32[2,512,8,128]{1,2,3,0:T(8,128)S(1)} fusion(f32[2,512,8,128]{1,3,2,0:T(8,128)S(1)} %bitcast.135), kind=kOutput, calls=%fused_computation.19.clone.1 | output fusion | flops 133169152 | bytes 8388608 | tf_op jit(solution)/shard_map/reduce-window
  95.3 2.0 copy-done
  97.4 2.7 %broadcast_add_fusion.2 = f32[2,512,8,128]{1,2,3,0:T(8,128)S(1)} fusion(f32[2,512,8,128]{1,2,3,0:T(8,128)} %copy-done, f32[2,512,8]{1,2,0:T(8,128)S(1)} %slice.847), kind=kLoop, calls=%fused_computation.22.clone.1 | loop fusion | flops 1048576 | bytes 8421376 | tf_op jit(solution)/shard_map/reduce_window_sum | solution.py:94
  100.1 2.4 %copy.44 = f32[2,512,8,128]{1,3,2,0:T(8,128)S(1)} copy(f32[2,512,8,128]{1,2,3,0:T(8,128)S(1)} %broadcast_add_fusion.2) | data formatting | bytes 8388608 | tf_op jit(solution)/shard_map/reduce_window_sum | solution.py:94
  102.5 6.9 %fusion.154 = bf16[2,512,1024]{1,2,0:T(8,128)(2,1)S(1)} fusion(f32[2,512,8,128]{1,3,2,0:T(8,128)S(1)} %copy.44, f32[2,1024,512]{2,1,0:T(8,128)S(1)} %copy-done.1, f32[2,512]{1,0:T(2,128)S(1)} %get-tuple-element.268, f32[2,1024]{1,0:T(2,128)S(1)} %dynamic-slice_convert_fusion.3, pred[512,1024]{0,1:T(8,128)(4,1)S(1)} %compare_and_fusion.2), kind=kLoop, calls=%fused_computation.7.clone.1 | loop fusion | flops 24117248 | bytes 11022336 | tf_op jit(solution)/shard_map/while/body/convert_element_type | solution.py:95
  110.7 0.7 dynamic-slice_convert_fusion.1
  111.5 3.2 %collective-permute-start = (f32[30,128]{1,0:T(8,128)S(1)}, f32[30,128]{1,0:T(8,128)S(1)}, u32[]{:S(2)}, u32[]{:S(2)}) collective-permute-start(f32[30,128]{1,0:T(8,128)S(1)} %slice.285), channel_id=1, source_target_pairs={{0,8},{8,16},{16,24},{1,9},{9,17},{17,25},{2,10},{10,18},{18,26},{... | collective-permute-start | bytes 46088 | tf_op jit(solution)/shard_map/ppermute | solution.py:18
  114.7 0.8 dynamic_slice.19
  115.9 1.1 fusion.130
  117.0 11.8 %all-reduce = (f32[512]{0:T(512)S(1)}, f32[512]{0:T(512)S(1)}) all-reduce(f32[512]{0:T(512)S(1)} %get-tuple-element.114, f32[512]{0:T(512)S(1)} %get-tuple-element.113), channel_id=1, replica_groups=mesh['sp'=4,'fs'=4,'tp'=2] {'fs','tp'}, use_global_device_ids=true, to_apply=%region_4.0 | all-reduce | flops 1024 | bytes 8192 | tf_op jit(solution)/shard_map/psum | solution.py:68
  128.8 0.9 multiply_convert_fusion
  129.7 35.2 %all-gather.10.cloned.1.call-done = bf16[512,1024]{0,1:T(8,128)(2,1)} async-done(((bf16[512,128]{0,1:T(8,128)(2,1)}), bf16[512,1024]{0,1:T(8,128)(2,1)}) %all-gather.10.cloned.1.call-update) | async-done | bytes 1048592 | tf_op jit(solution)/shard_map/all_gather | solution.py:129
  164.9 1.5 fusion.23
  166.4 2.0 %convolution_multiply_fusion = f32[512,256]{1,0:T(8,128)S(1)} fusion(bf16[512,1024]{0,1:T(8,128)(2,1)} %all-gather.10.cloned.1.call-done, f32[1024]{0:T(1024)S(1)} %copy-done.5, bf16[2048,256]{1,0:T(8,128)(2,1)} %param.27, f32[512]{0:T(512)S(1)} %add_rsqrt_fusion), kind=kOutput, calls=%fused_computation.79 | convolution fusion | flops 270139392 | bytes 2103296 | tf_op jit(solution)/shard_map/dot_general | solution.py:138
  168.5 21.8 %all-gather.8.cloned.1.call-done = bf16[512,1024]{1,0:T(8,128)(2,1)} async-done(((bf16[512,128]{1,0:T(8,128)(2,1)}), bf16[512,1024]{1,0:T(8,128)(2,1)}) %all-gather.8.cloned.1.call-update) | async-done | bytes 1048592 | tf_op jit(solution)/shard_map/all_gather | solution.py:128
  190.3 1.5 fusion.21
  191.8 2.4 %fusion.34 = bf16[512,256]{1,0:T(8,128)(2,1)} fusion(f32[512,256]{1,0:T(8,128)S(1)} %convolution_multiply_fusion, bf16[512,1024]{1,0:T(8,128)(2,1)} %all-gather.8.cloned.1.call-done, f32[1024]{0:T(1024)S(1)} %copy-done.6, bf16[2048,256]{1,0:T(8,128)(2,1)S(1)} %copy-done.3, f32[512]{0:T(512)S(1)} %add_rsqrt_fusion.1), kind=kOutput, calls=%fused_computation.82 | convolution fusion | flops 270401536 | bytes 2365440 | tf_op jit(solution)/shard_map/dot_general | solution.py:137
  (44 shorter events, 2.5 us)
Async XLA Ops:
  6.5 22.2 %copy-start.2 = (bf16[2048,128]{1,0:T(8,128)(2,1)S(1)}, bf16[2048,128]{1,0:T(8,128)(2,1)}, u32[]{:S(2)}) copy-start(bf16[2048,128]{1,0:T(8,128)(2,1)} %param.21) | copy-start | bytes 1572868
  6.5 35.6 %copy-start.4 = (f32[2048]{0:T(1024)S(1)}, f32[2048]{0:T(1024)}, u32[]{:S(2)}) copy-start(f32[2048]{0:T(1024)} %param.16) | copy-start | bytes 24580
  6.5 33.5 %all-gather.6.cloned.1.call-start = ((), (), s32[]{:S(2)}) async-start(), calls=%async_computation | async-start | bytes 2359296 | tf_op jit(solution)/shard_map/all_gather | solution.py:46
  7.3 157.6 %all-gather.10.cloned.1.call-start = ((), (), s32[]{:S(2)}) async-start(), calls=%async_computation.2 | async-start | bytes 1179648 | tf_op jit(solution)/shard_map/all_gather | solution.py:129
  78.7 87.8 %copy-start.5 = (f32[1024]{0:T(1024)S(1)}, f32[1024]{0:T(1024)}, u32[]{:S(2)}) copy-start(f32[1024]{0:T(1024)} %param.26) | copy-start | bytes 12292
  95.3 2.0 copy-start
  100.1 2.4 %copy-start.1 = (f32[2,1024,512]{2,1,0:T(8,128)S(1)}, f32[2,1024,512]{2,1,0:T(8,128)}, u32[]{:S(2)}) copy-start(f32[2,1024,512]{2,1,0:T(8,128)} %get-tuple-element.249) | copy-start | bytes 12582916 | tf_op jit(solution)/shard_map/while
  109.9 81.9 %copy-start.3 = (bf16[2048,256]{1,0:T(8,128)(2,1)S(1)}, bf16[2048,256]{1,0:T(8,128)(2,1)}, u32[]{:S(2)}) copy-start(bf16[2048,256]{1,0:T(8,128)(2,1)} %param.27) | copy-start | bytes 3145732
  109.9 81.9 %copy-start.6 = (f32[1024]{0:T(1024)S(1)}, f32[1024]{0:T(1024)}, u32[]{:S(2)}) copy-start(f32[1024]{0:T(1024)} %param.25) | copy-start | bytes 12292
  110.6 79.7 %all-gather.8.cloned.1.call-start = ((), (), s32[]{:S(2)}) async-start(), calls=%async_computation.1 | async-start | bytes 1179648 | tf_op jit(solution)/shard_map/all_gather | solution.py:128
  111.5 4.4 %collective-permute-start = (f32[30,128]{1,0:T(8,128)S(1)}, f32[30,128]{1,0:T(8,128)S(1)}, u32[]{:S(2)}, u32[]{:S(2)}) collective-permute-start(f32[30,128]{1,0:T(8,128)S(1)} %slice.285), channel_id=1, source_target_pairs={{0,8},{8,16},{16,24},{1,9},{9,17},{17,25},{2,10},{10,18},{18,26},{... | collective-permute-start | bytes 46088 | tf_op jit(solution)/shard_map/ppermute | solution.py:18
Sparse Core Ops, SparseCore 0:
  9.2 30.8 all-gather.5
  110.7 54.1 all-gather.9
  166.8 23.4 all-gather.7
